TPU v7x, 32 devices: a whole 2x2x4 slice. The times are simulated.
32 devices in a mesh: sp: 8 (over z, core), tp: 4 (over y, x).
Axes of the slice: x: 2, y: 2, z: 4, core: 2. Of those that a mesh axis runs over, the one named last changes fastest.
Arguments:
- residual: bfloat16 [1024, 2048], P('sp', 'tp'), may hold values from -48 to 48
- glu_value: bfloat16 [1024, 2048], P('sp', 'tp'), may hold values from -48 to 48
- glu_gate: bfloat16 [1024, 2048], P('sp', 'tp'), may hold values from -6 to 6
- conv_weight: bfloat16 [31, 2048], P(None, 'tp'), may hold values from -1 to 1
- conv_bias: float32 [2048], P('tp'), may hold values from -3 to 3
- ln_gain: float32 [2048], P('tp'), may hold values from 0.1 to 1.9
- ln_bias: float32 [2048], P('tp'), may hold values from -3 to 3
- out_weight: bfloat16 [2048, 2048], P(None, 'tp'), may hold values from -0.125 to 0.125
- norm_gain: float32 [2048], P('tp'), may hold values from 0.1 to 1.9
- route_ids: int32 [1024, 2], P('sp'), may hold values from 0 to 7, all different within a row; in each aligned block of 128 rows (0 to 127, 128 to 255, ...) at most 64 rows name the same one
- route_weight: float32 [1024, 2], P('sp'), may hold values from 0.1 to 1
- expert_gate: bfloat16 [8, 2048, 4096], P('sp', None, 'tp'), may hold values from -0.125 to 0.125
- expert_up: bfloat16 [8, 2048, 4096], P('sp', None, 'tp'), may hold values from -0.125 to 0.125
- expert_down: bfloat16 [8, 4096, 2048], P('sp', 'tp'), may hold values from -0.09375 to 0.09375
Outputs:
- layer_out: bfloat16 [1024, 2048], P('sp', 'tp')
Inputs may be any that keep to these rules, and one draw needn't show every extreme that they name: `route_ids`: within the 128 rows of one index of sp, no expert is named more than 64 times, and in some such rows one expert is named exactly 64 times.
All inputs are finite; a program needn't handle non-finite values.
Results may differ from a plain program's by a relative error of at most 0.006.
Values may be sent and summed in bfloat16 or wider, within the bound.
No kernel may reach another device: no remote copies, remote signals or barrier semaphores. Data moves between devices by JAX's collectives and lax.ppermute only.
A program may use at most 64 MiB of HBM per device.

v0:
```python
import jax
import jax.numpy as jnp
from jax import lax
from jax.sharding import PartitionSpec as P

TOPK = 2


def with_halo(cells, sides, width):
    for axis, dim in sides:
        count = lax.axis_size(axis)
        ends = count - 1
        head = lax.slice_in_dim(cells, 0, width, axis=dim)
        tail = lax.slice_in_dim(cells, cells.shape[dim] - width, cells.shape[dim], axis=dim)
        cells = jnp.concatenate(
            [
                lax.ppermute(tail, axis, [(i, (i + 1) % count) for i in range(ends)]),
                cells,
                lax.ppermute(head, axis, [((i + 1) % count, i) for i in range(ends)]),
            ],
            axis=dim,
        )
    return cells


def on_device(
    residual,
    glu_value,
    glu_gate,
    conv_weight,
    conv_bias,
    ln_gain,
    ln_bias,
    out_weight,
    norm_gain,
    route_ids,
    route_weight,
    expert_gate,
    expert_up,
    expert_down,
):
    rows = residual.shape[0]
    width_all = out_weight.shape[0]
    gated = (glu_value.astype(jnp.float32) * jax.nn.sigmoid(glu_gate.astype(jnp.float32))).astype(
        jnp.bfloat16
    )
    reach = conv_weight.shape[0] // 2
    padded = with_halo(gated, (("sp", 0),), reach)
    taps = conv_weight.astype(jnp.float32)
    conv = jnp.zeros(gated.shape, jnp.float32) + conv_bias
    for tap in range(conv_weight.shape[0]):
        conv = conv + padded[tap : tap + rows].astype(jnp.float32) * taps[tap]
    totals = lax.psum((jnp.sum(conv, axis=1), jnp.sum(conv * conv, axis=1)), "tp")
    mean = (totals[0] / width_all)[:, None]
    var = (totals[1] / width_all)[:, None] - mean * mean
    act = jax.nn.silu((conv - mean) * lax.rsqrt(var + 1e-05) * ln_gain + ln_bias).astype(
        jnp.bfloat16
    )
    projected = jnp.dot(
        lax.all_gather(act, "tp", axis=1, tiled=True),
        out_weight,
        preferred_element_type=jnp.float32,
    )
    mixed = residual.astype(jnp.float32) + projected
    squares = lax.psum(jnp.sum(mixed * mixed, axis=1), "tp")
    normed = (mixed * lax.rsqrt(squares / width_all + 1e-06)[:, None] * norm_gain).astype(
        jnp.bfloat16
    )
    experts = lax.axis_size("sp")
    capacity = 2 * rows * TOPK // experts
    flat = route_ids.reshape(-1)
    onehot = (flat[:, None] == jnp.arange(experts, dtype=jnp.int32)[None, :]).astype(jnp.int32)
    rank = jnp.sum((jnp.cumsum(onehot, axis=0) - 1) * onehot, axis=1)
    slot_of = flat * capacity + rank
    placing = (slot_of[None, :] == jnp.arange(experts * capacity, dtype=jnp.int32)[:, None]).astype(
        jnp.bfloat16
    )
    copies = jnp.repeat(normed, TOPK, axis=0)
    outgoing = jnp.dot(placing, copies, preferred_element_type=jnp.float32).astype(jnp.bfloat16)
    outgoing = outgoing.reshape(experts, capacity, normed.shape[1])
    arrived = lax.all_to_all(outgoing, "sp", split_axis=0, concat_axis=0, tiled=True)
    arrived = lax.all_gather(
        arrived.reshape(experts * capacity, normed.shape[1]), "tp", axis=1, tiled=True
    )
    gate = jnp.dot(arrived, expert_gate[0], preferred_element_type=jnp.float32)
    up = jnp.dot(arrived, expert_up[0], preferred_element_type=jnp.float32)
    hidden = (jax.nn.silu(gate) * up).astype(jnp.bfloat16)
    partial_out = jnp.dot(hidden, expert_down[0], preferred_element_type=jnp.float32)
    summed = lax.psum_scatter(
        partial_out.astype(jnp.bfloat16), "tp", scatter_dimension=1, tiled=True
    )
    summed = summed.reshape(experts, capacity, summed.shape[1])
    returned = lax.all_to_all(summed, "sp", split_axis=0, concat_axis=0, tiled=True)
    returned = returned.reshape(experts * capacity, returned.shape[2])
    picked = lax.dot_general(
        placing, returned, (((0,), (0,)), ((), ())), preferred_element_type=jnp.float32
    )
    picked = picked.reshape(rows, TOPK, picked.shape[1])
    moe = jnp.sum(picked * route_weight[:, :, None], axis=1)
    return (mixed + moe).astype(jnp.bfloat16)


def solution(mesh):
    in_specs = (
        P("sp", "tp"),
        P("sp", "tp"),
        P("sp", "tp"),
        P(None, "tp"),
        P("tp"),
        P("tp"),
        P("tp"),
        P(None, "tp"),
        P("tp"),
        P("sp", None),
        P("sp", None),
        P("sp", None, "tp"),
        P("sp", None, "tp"),
        P("sp", "tp", None),
    )
    out_specs = P("sp", "tp")
    return jax.shard_map(
        on_device, mesh=mesh, in_specs=in_specs, out_specs=out_specs, check_vma=False
    )
```

profile of v0, /device:TPU:0, one launch (start us, length us, event | category | flops | bytes accessed | tf_op | source)
XLA Modules:
  0.0 184.5 jit_solution(897781840962571341)
XLA Ops:
  6.5 0.0 copy-start
  6.5 0.0 copy-start.1
  6.5 0.0 all-gather.2.cloned.1.call-start
  6.5 1.2 multiply_convert_fusion.3
  7.8 2.4 %collective-permute-start = (bf16[15,512]{1,0:T(8,128)(2,1)S(1)}, bf16[15,512]{1,0:T(8,128)(2,1)S(1)}, u32[]{:S(2)}, u32[]{:S(2)}) collective-permute-start(bf16[15,512]{1,0:T(8,128)(2,1)S(1)} %get-tuple-element.10), channel_id=1, source_target_pairs={{0,4},{4,8},{8,12},{12,16},{16,20},{20,24},{24,28},{1,5},{5,9},{9,... | collective-permute-start | bytes 46088 | tf_op jit(solution)/shard_map/ppermute | solution.py:17
  10.2 1.3 collective-permute-start.1
  11.5 1.0 fusion.52
  12.4 1.0 fusion.51
  13.5 0.8 copy.20
  14.3 0.1 reshape.76
  14.4 0.1 eq.58
  14.6 0.6 reduce-window.6
  15.2 0.2 slice_reduce_fusion
  15.4 0.1 fusion.46
  15.5 0.0 collective-permute-done
  15.5 0.0 collective-permute-done.1
  15.5 2.0 %fusion.49 = (f32[128]{0:T(128)S(1)}, f32[128]{0:T(128)S(1)}, f32[128,512]{1,0:T(8,128)S(1)}) fusion(f32[512]{0:T(512)S(1)} %bitcast.82, bf16[15,512]{1,0:T(8,128)(2,1)S(1)} %collective-permute-done.1, bf16[128,512]{1,0:T(8,128)(2,1)S(1)} %multiply_convert_fusion.3, f32[512]{0:T(512)S(1)} %bitcast.81, f32[512]{0:T(512)S(1)} %bitcast.80, ...), kind=kLoop, calls=%fused_computation.114 | loop fusion | flops 12189440 | bytes 490496 | tf_op jit(solution)/shard_map/reduce_sum | solution.py:53
  17.5 0.0 copy-start.3
  17.5 10.7 %all-reduce = (f32[128]{0:T(128)S(1)}, f32[128]{0:T(128)S(1)}) all-reduce(f32[128]{0:T(128)S(1)} %get-tuple-element.6, f32[128]{0:T(128)S(1)} %get-tuple-element.5), channel_id=1, replica_groups=mesh['sp'=8,'tp'=4] {'tp'}, use_global_device_ids=true, to_apply=%region_3.0 | all-reduce | flops 256 | bytes 2048 | tf_op jit(solution)/shard_map/psum | solution.py:53
  28.3 0.9 multiply_convert_fusion.2
  29.2 9.6 %all_gather.6 = bf16[128,2048]{1,0:T(8,128)(2,1)S(1)} all-gather(bf16[128,512]{1,0:T(8,128)(2,1)S(1)} %multiply_convert_fusion.2), channel_id=1, replica_groups=mesh['sp'=8,'tp'=4] {'tp'}, dimensions={1}, use_global_device_ids=true | all-gather | bytes 655360 | tf_op jit(solution)/shard_map/all_gather | solution.py:60
  38.8 0.0 copy-done
  38.8 0.0 copy-done.1
  38.8 0.6 multiply_reduce_fusion
  39.3 8.9 %psum.23 = f32[128]{0:T(128)S(1)} all-reduce(f32[128]{0:T(128)S(1)} %get-tuple-element.45), channel_id=1, replica_groups=mesh['sp'=8,'tp'=4] {'tp'}, use_global_device_ids=true, to_apply=%region_8.9 | all-reduce | flops 128 | bytes 1024 | tf_op jit(solution)/shard_map/psum | solution.py:65
  48.3 0.0 copy-done.3
  48.3 0.1 multiply_convert_fusion.1
  48.4 0.1 broadcast_in_dim.2
  48.5 0.1 reshape.78
  48.7 0.3 convolution_convert_fusion
  49.0 22.2 %all_to_all.10 = bf16[8,64,512]{2,1,0:T(8,128)(2,1)} all-to-all(bf16[8,64,512]{2,1,0:T(8,128)(2,1)S(1)} %bitcast.68), channel_id=1, replica_groups=mesh['sp'=8,'tp'=4] {'sp'}, dimensions={0} | all-to-all | bytes 1048576 | tf_op jit(solution)/shard_map/all_to_all | solution.py:81
  71.2 0.0 all-gather.2.cloned.1.call-update
  71.2 0.0 reduce-scatter.2.cloned.1.call-start
  71.2 33.1 %all-gather.2.cloned.1.call-done = bf16[512,2048]{1,0:T(8,128)(2,1)} async-done(((bf16[512,512]{1,0:T(8,128)(2,1)}), bf16[512,2048]{1,0:T(8,128)(2,1)}) %all-gather.2.cloned.1.call-update) | async-done | bytes 2097168 | tf_op jit(solution)/shard_map/all_gather | solution.py:82
  104.3 6.5 %fusion.4 = f32[512,1024]{1,0:T(8,128)} fusion(bf16[512,2048]{1,0:T(8,128)(2,1)} %all-gather.2.cloned.1.call-done, bf16[1,2048,1024]{2,1,0:T(8,128)(2,1)} %param.25), kind=kOutput, calls=%fused_computation.4 | convolution fusion | flops 2147483648 | bytes 8388608 | tf_op jit(solution)/shard_map/dot_general | solution.py:85
  110.8 10.5 %fusion.6 = bf16[512,2048]{1,0:T(8,128)(2,1)} fusion(bf16[1,1024,2048]{2,1,0:T(8,128)(2,1)} %param.27, f32[512,1024]{1,0:T(8,128)} %fusion.4, bf16[512,2048]{1,0:T(8,128)(2,1)} %all-gather.2.cloned.1.call-done, bf16[1,2048,1024]{2,1,0:T(8,128)(2,1)} %param.26), kind=kOutput, calls=%fused_computation.6 | convolution fusion | flops 4299161600 | bytes 14680064 | tf_op jit(solution)/shard_map/dot_general | solution.py:88
  121.4 0.0 copy-start.2
  121.4 0.0 copy-start.4
  121.4 0.0 reduce-scatter.2.cloned.1.call-update
  121.4 35.3 %reduce-scatter.2.cloned.1.call-done = bf16[512,512]{1,0:T(8,128)(2,1)} async-done(((bf16[512,2048]{1,0:T(8,128)(2,1)}), bf16[512,512]{1,0:T(8,128)(2,1)}) %reduce-scatter.2.cloned.1.call-update) | async-done | bytes 524304 | tf_op jit(solution)/shard_map/reduce_scatter | solution.py:89
  156.7 4.6 %all-to-all-start.1 = ((bf16[8,64,512]{2,1,0:T(8,128)(2,1)}), bf16[8,64,512]{2,1,0:T(8,128)(2,1)S(1)}, u32[]{:S(2)}, u32[]{:S(2)}) async-start(bf16[8,64,512]{2,1,0:T(8,128)(2,1)} %bitcast.69), calls=%async_computation.2 | async-start | bytes 1048576 | tf_op jit(solution)/shard_map/all_to_all | solution.py:93
  161.3 0.1 reduce_sum.50
  161.5 0.1 copy.22
  161.5 0.0 copy-done.2
  161.5 15.1 %all-to-all-done.1 = bf16[8,64,512]{2,1,0:T(8,128)(2,1)S(1)} async-done(((bf16[8,64,512]{2,1,0:T(8,128)(2,1)}), bf16[8,64,512]{2,1,0:T(8,128)(2,1)S(1)}, u32[]{:S(2)}, u32[]{:S(2)}) %all-to-all-start.1) | async-done | bytes 524320 | tf_op jit(solution)/shard_map/all_to_all | solution.py:93
  176.7 0.0 copy-done.4
  176.7 0.3 fusion.11
  177.0 0.7 add_convert_fusion
  (8 shorter events, 0.1 us)
Async XLA Ops:
  6.5 32.2 %copy-start = (bf16[2048,512]{1,0:T(8,128)(2,1)S(1)}, bf16[2048,512]{1,0:T(8,128)(2,1)}, u32[]{:S(2)}) copy-start(bf16[2048,512]{1,0:T(8,128)(2,1)} %param.21) | copy-start | bytes 6291460
  6.5 32.2 %copy-start.1 = (bf16[128,512]{1,0:T(8,128)(2,1)S(1)}, bf16[128,512]{1,0:T(8,128)(2,1)}, u32[]{:S(2)}) copy-start(bf16[128,512]{1,0:T(8,128)(2,1)} %param.14) | copy-start | bytes 393220
  6.5 97.8 %all-gather.2.cloned.1.call-start = ((), (), s32[]{:S(2)}) async-start(), calls=%async_computation.3 | async-start | bytes 2621440 | tf_op jit(solution)/shard_map/all_gather | solution.py:82
  7.8 7.8 %collective-permute-start = (bf16[15,512]{1,0:T(8,128)(2,1)S(1)}, bf16[15,512]{1,0:T(8,128)(2,1)S(1)}, u32[]{:S(2)}, u32[]{:S(2)}) collective-permute-start(bf16[15,512]{1,0:T(8,128)(2,1)S(1)} %get-tuple-element.10), channel_id=1, source_target_pairs={{0,4},{4,8},{8,12},{12,16},{16,20},{20,24},{24,28},{1,5},{5,9},{9,... | collective-permute-start | bytes 46088 | tf_op jit(solution)/shard_map/ppermute | solution.py:17
  10.2 5.4 %collective-permute-start.1 = (bf16[15,512]{1,0:T(8,128)(2,1)S(1)}, bf16[15,512]{1,0:T(8,128)(2,1)S(1)}, u32[]{:S(2)}, u32[]{:S(2)}) collective-permute-start(bf16[15,512]{1,0:T(8,128)(2,1)S(1)} %get-tuple-element.11), channel_id=1, source_target_pairs={{4,0},{8,4},{12,8},{16,12},{20,16},{24,20},{28,24},{5,1},{9,5},{13... | collective-permute-start | bytes 46088 | tf_op jit(solution)/shard_map/ppermute | solution.py:19
  17.5 30.8 %copy-start.3 = (f32[512]{0:T(512)S(1)}, f32[512]{0:T(512)}, u32[]{:S(2)}) copy-start(f32[512]{0:T(512)} %param.22) | copy-start | bytes 6148
  71.2 85.5 %reduce-scatter.2.cloned.1.call-start = ((), (), s32[]{:S(2)}) async-start(), calls=%async_computation.4 | async-start | bytes 2621440 | tf_op jit(solution)/shard_map/reduce_scatter | solution.py:89
  121.4 40.2 %copy-start.2 = (s32[128,2]{0,1:T(2,128)S(1)}, s32[128,2]{0,1:T(2,128)}, u32[]{:S(2)}) copy-start(s32[128,2]{0,1:T(2,128)} %param.23) | copy-start | bytes 3076
  121.4 55.3 %copy-start.4 = (f32[128,2]{0,1:T(2,128)S(1)}, f32[128,2]{0,1:T(2,128)}, u32[]{:S(2)}) copy-start(f32[128,2]{0,1:T(2,128)} %param.24) | copy-start | bytes 3076
  156.7 19.9 %all-to-all-start.1 = ((bf16[8,64,512]{2,1,0:T(8,128)(2,1)}), bf16[8,64,512]{2,1,0:T(8,128)(2,1)S(1)}, u32[]{:S(2)}, u32[]{:S(2)}) async-start(bf16[8,64,512]{2,1,0:T(8,128)(2,1)} %bitcast.69), calls=%async_computation.2 | async-start | bytes 1048576 | tf_op jit(solution)/shard_map/all_to_all | solution.py:93
Sparse Core Ops, SparseCore 0:
  71.3 32.9 all-gather.1
  121.5 35.1 reduce-scatter.1
where the time goes:
time: 185 us
  waiting for transfers between devices  83.6 us (45%)
  blocking collectives  51.5 us (28%)
  matrix products  18.2 us (10%)
  between operations  13.6 us (7%)
  starting transfers between devices  8.34 us (5%)
  other arithmetic  5.59 us (3%)
  local copies, waits for them, and re-layouts  3.76 us (2%)
    reduce_scatter x1, waiting for transfers between devices, on_device(): lax.psum_scatter(partial_out.astype(jnp.bfloat16), 'tp', scatter_dimensio...  35.3 us
    all_gather x1, waiting for transfers between devices, on_device(): lax.all_gather(arrived.reshape(experts * capacity, normed.shape[1]), 'tp'...  33.1 us
    all_to_all x1, blocking collectives, on_device(): lax.all_to_all(outgoing, 'sp', split_axis=0, concat_axis=0, tiled=True)  22.2 us
    all_to_all x1, waiting for transfers between devices, on_device(): lax.all_to_all(summed, 'sp', split_axis=0, concat_axis=0, tiled=True)  15.1 us
    psum x1, blocking collectives, on_device(): lax.psum((jnp.sum(conv, axis=1), jnp.sum(conv * conv, axis=1)), 'tp')  10.7 us
    dot_general x1, matrix products, on_device(): jnp.dot(hidden, expert_down[0], preferred_element_type=jnp.float32)  10.5 us
    all_gather x1, blocking collectives, on_device(): lax.all_gather(act, 'tp', axis=1, tiled=True)  9.61 us
    psum x1, blocking collectives, on_device(): squares = lax.psum(jnp.sum(mixed * mixed, axis=1), 'tp')  8.93 us
  transfers between devices with their start and end apart: 5, of which 3 were waited for; matrix products, arithmetic and copies ran while one was open for 2% of the time, Pallas kernels for 0%

commit v1 on v0

v1 whole, which is shorter than its diff:
```python
import functools

import jax
import jax.numpy as jnp
from jax import lax
from jax.experimental import pallas as pl
from jax.experimental.pallas import tpu as pltpu
from jax.sharding import PartitionSpec as P

F32 = jnp.float32
BF16 = jnp.bfloat16
SUB = 16
LANES = 128
VMEM_SPEC = pl.BlockSpec(memory_space=pltpu.VMEM)
SMEM_SPEC = pl.BlockSpec(memory_space=pltpu.SMEM)


def swap(value, axis, offset):
    count = lax.axis_size(axis)
    return lax.ppermute(value, axis, [(i, i ^ offset) for i in range(count)])


def spread(value, axis):
    return [value] + [swap(value, axis, k) for k in range(1, lax.axis_size(axis))]


def route_kernel(here, ids, slots_col, slots_row, *, capacity):
    rows = ids.shape[0]
    topk = ids.shape[1]
    lane = lax.broadcasted_iota(jnp.int32, (rows, LANES), 1)
    row = lax.broadcasted_iota(jnp.int32, (rows, rows), 0)
    col = lax.broadcasted_iota(jnp.int32, (rows, rows), 1)
    earlier = jnp.where(col < row, 1.0, 0.0).astype(BF16)
    hits = [jnp.where(lane == ids[:, k : k + 1], 1.0, 0.0) for k in range(topk)]
    before = jnp.dot(earlier, sum(hits).astype(BF16), preferred_element_type=F32)
    rowform = []
    colform = jnp.zeros((rows, LANES), jnp.int32)
    for k in range(topk):
        rank = jnp.sum(before * hits[k], axis=1, keepdims=True).astype(jnp.int32)
        slot = (ids[:, k : k + 1] ^ here[0]) * capacity + rank
        colform = jnp.where(lane == k, slot, colform)
        wide = jnp.broadcast_to(slot.astype(F32), (rows, rows))
        rowform.append(wide.T[:8].astype(jnp.int32))
    slots_col[...] = colform
    sub = lax.broadcasted_iota(jnp.int32, (8, rows), 0)
    out = rowform[0]
    for k in range(1, topk):
        out = jnp.where(sub == k, rowform[k], out)
    slots_row[...] = out


def conv_kernel(before, gated, after, taps, bias, gain, shift, scale, out, padded):
    rows, width = gated.shape
    edge = before.shape[0]
    count = taps.shape[0]
    reach = count // 2
    padded[:edge] = before[...].astype(F32)
    padded[edge : edge + rows] = gated[...].astype(F32)
    padded[edge + rows :] = after[...].astype(F32)
    first = edge - reach
    sums = jnp.zeros((rows, LANES), F32)
    pieces = []
    for lo in range(0, width, LANES):
        part = slice(lo, lo + LANES)
        weights = taps[:, part].astype(F32)
        acc = jnp.broadcast_to(bias[:, part], (rows, LANES))
        for turn in range(8):
            mine = [t for t in range(count) if (t + first) % 8 == turn]
            if not mine:
                continue
            top = max((t + first) // 8 for t in mine) * 8
            moved = padded[turn : turn + top + rows, part]
            for t in mine:
                at = (t + first) // 8 * 8
                acc = acc + moved[at : at + rows] * weights[t : t + 1]
        pieces.append(acc)
        sums = sums + acc
    mean = jnp.sum(sums, axis=1, keepdims=True) * (1.0 / width)
    pivot = mean.astype(BF16).astype(F32)
    for i, acc in enumerate(pieces):
        out[:rows, i * LANES : (i + 1) * LANES] = (acc - pivot).astype(BF16)
    line = jnp.broadcast_to(pivot, (rows, rows)).T[:SUB]
    sub = lax.broadcasted_iota(jnp.int32, (SUB, width), 0)
    if width > rows:
        line = jnp.concatenate([line, jnp.zeros((SUB, width - rows), F32)], axis=1)
    tail = line
    at = 1
    for vector in (gain, shift, scale):
        left = vector[...]
        for _ in range(3):
            piece = left.astype(BF16).astype(F32)
            tail = jnp.where(sub == at, piece, tail)
            left = left - piece
            at += 1
    out[rows:] = jnp.where(sub < at, tail, 0.0).astype(BF16)


def mix_kernel(here, *refs, peers, spots, capacity, topk):
    exts = refs[:peers]
    weight, residual, slots_row, mixed_out, inverse = refs[peers : peers + 5]
    outgoing = refs[peers + 5 :]
    rows, width = residual.shape
    total = width * peers
    sums = jnp.zeros((rows, LANES), F32)
    pivots = []
    for k in range(peers):
        line = exts[k][rows : rows + 8, :rows].astype(F32)[:1]
        pivot = jnp.broadcast_to(line, (rows, rows)).T[:, :1]
        pivots.append(pivot)
        part = exts[k][:rows].astype(F32)
        for lo in range(0, width, LANES):
            sums = sums + part[:, lo : lo + LANES]
    mean = jnp.sum(sums, axis=1, keepdims=True) * (1.0 / total)
    mean = mean + sum(pivots) * (1.0 / peers)
    squares = jnp.zeros((rows, LANES), F32)
    for k in range(peers):
        part = exts[k][:rows].astype(F32) + (pivots[k] - mean)
        part = part * part
        for lo in range(0, width, LANES):
            squares = squares + part[:, lo : lo + LANES]
    var = jnp.sum(squares, axis=1, keepdims=True) * (1.0 / total)
    rate = lax.rsqrt(var + 1e-05)
    acc = residual[...].astype(F32)
    rowid = lax.broadcasted_iota(jnp.int32, (inverse.shape[0], width), 0)
    inverses = jnp.zeros((inverse.shape[0], width), F32)
    own_scale = None
    for k in range(peers):
        extra = exts[k][rows:].astype(F32)
        gain = extra[1:2] + extra[2:3] + extra[3:4]
        shift = extra[4:5] + extra[5:6] + extra[6:7]
        scale = extra[7:8] + extra[8:9] + extra[9:10]
        if k == 0:
            own_scale = scale
        inverses = jnp.where(rowid == k, 1.0 / scale, inverses)
        pre = (exts[k][:rows].astype(F32) + (pivots[k] - mean)) * rate * gain + shift
        act = (pre / (1.0 + jnp.exp(-pre))).astype(BF16)
        start = pl.multiple_of((here[1] ^ k) * width, width)
        acc = acc + jnp.dot(act, weight[pl.ds(start, width), :], preferred_element_type=F32)
    inverse[...] = inverses
    mixed_out[...] = acc
    scaled = (acc * own_scale).astype(BF16)
    for d in range(spots):
        slot = lax.broadcasted_iota(jnp.int32, (capacity, rows), 0) + d * capacity
        match = slot == slots_row[0:1]
        for j in range(1, topk):
            match = match | (slot == slots_row[j : j + 1])
        chosen = jnp.where(match, 1.0, 0.0).astype(BF16)
        outgoing[d][...] = jnp.dot(chosen, scaled, preferred_element_type=F32).astype(BF16)


def ffn_kernel(here, *refs, peers):
    blocks = refs[:peers]
    inverse, gate_w, up_w, down_w = refs[peers : peers + 4]
    outs = refs[peers + 4 : 2 * peers + 4]
    gate_acc, up_acc, square_acc, hidden = refs[2 * peers + 4 :]
    step = pl.program_id(0)
    width = blocks[0].shape[1]
    for k in range(peers):

        @pl.when(step == k)
        def _(k=k):
            x = blocks[k][...]
            gate = jnp.dot(x, gate_w[...], preferred_element_type=F32)
            up = jnp.dot(x, up_w[...], preferred_element_type=F32)
            plain = x.astype(F32) * inverse[k : k + 1]
            plain = plain * plain
            folded = plain[:, :LANES]
            for lo in range(LANES, width, LANES):
                folded = folded + plain[:, lo : lo + LANES]
            if k == 0:
                gate_acc[...] = gate
                up_acc[...] = up
                square_acc[...] = folded
            else:
                gate_acc[...] += gate
                up_acc[...] += up
                square_acc[...] += folded

    @pl.when(step == peers)
    def _():
        squares = jnp.sum(square_acc[...], axis=1, keepdims=True)
        rate = lax.rsqrt(squares * (1.0 / (width * peers)) + 1e-06)
        gate = gate_acc[...] * rate
        up = up_acc[...] * rate
        hidden[...] = (gate / (1.0 + jnp.exp(-gate)) * up).astype(BF16)

    for k in range(peers):

        @pl.when(step == peers + k)
        def _(k=k):
            outs[k][...] = jnp.dot(hidden[...], down_w[...], preferred_element_type=F32).astype(
                BF16
            )


def combine_kernel(*refs, spots, topk):
    pieces = refs[:spots]
    slots_col, weights, mixed, out = refs[spots:]
    rows = mixed.shape[0]
    capacity = pieces[0].shape[0]
    table = jnp.concatenate([piece[...] for piece in pieces], axis=0)
    slot = lax.broadcasted_iota(jnp.int32, (rows, spots * capacity), 1)
    total = mixed[...]
    for k in range(topk):
        chosen = jnp.where(slot == slots_col[:, k : k + 1], 1.0, 0.0).astype(BF16)
        picked = jnp.dot(chosen, table, preferred_element_type=F32)
        total = total + picked * weights[:, k : k + 1]
    out[...] = total.astype(BF16)


def on_device(
    residual,
    glu_value,
    glu_gate,
    conv_weight,
    conv_bias,
    ln_gain,
    ln_bias,
    out_weight,
    norm_gain,
    route_ids,
    route_weight,
    expert_gate,
    expert_up,
    expert_down,
):
    rows, width = residual.shape
    spots = lax.axis_size("sp")
    peers = lax.axis_size("tp")
    topk = route_ids.shape[1]
    capacity = 2 * rows * topk // spots
    hidden_units = expert_gate.shape[2]
    here = jnp.stack([lax.axis_index("sp"), lax.axis_index("tp")]).astype(jnp.int32)

    gated = (glu_value.astype(F32) * jax.nn.sigmoid(glu_gate.astype(F32))).astype(BF16)
    reach = conv_weight.shape[0] // 2
    edge = -(-reach // SUB) * SUB
    ends = spots - 1
    before = lax.ppermute(gated[rows - edge :], "sp", [(i, i + 1) for i in range(ends)])
    after = lax.ppermute(gated[:edge], "sp", [(i + 1, i) for i in range(ends)])

    slots_col, slots_row = pl.pallas_call(
        functools.partial(route_kernel, capacity=capacity),
        out_shape=(
            jax.ShapeDtypeStruct((rows, LANES), jnp.int32),
            jax.ShapeDtypeStruct((8, rows), jnp.int32),
        ),
        in_specs=[SMEM_SPEC, VMEM_SPEC],
        out_specs=(VMEM_SPEC, VMEM_SPEC),
        name="route",
    )(here, route_ids)

    ext = pl.pallas_call(
        conv_kernel,
        out_shape=jax.ShapeDtypeStruct((rows + SUB, width), BF16),
        in_specs=[VMEM_SPEC] * 8,
        out_specs=VMEM_SPEC,
        scratch_shapes=[pltpu.VMEM((rows + 2 * edge, width), F32)],
        name="conv",
    )(
        before,
        gated,
        after,
        conv_weight,
        conv_bias[None],
        ln_gain[None],
        ln_bias[None],
        norm_gain[None],
    )
    exts = spread(ext, "tp")

    padded_peers = -(-peers // 8) * 8
    mixed, inverse, *outgoing = pl.pallas_call(
        functools.partial(
            mix_kernel, peers=peers, spots=spots, capacity=capacity, topk=topk
        ),
        out_shape=[
            jax.ShapeDtypeStruct((rows, width), F32),
            jax.ShapeDtypeStruct((padded_peers, width), F32),
        ]
        + [jax.ShapeDtypeStruct((capacity, width), BF16)] * spots,
        in_specs=[SMEM_SPEC] + [VMEM_SPEC] * (peers + 3),
        out_specs=[VMEM_SPEC] * (spots + 2),
        name="mix",
    )(here, *exts, out_weight, residual, slots_row)

    arrived = [outgoing[0]] + [swap(outgoing[d], "sp", d) for d in range(1, spots)]

    def expert(chunk):
        blocks = spread(chunk, "tp")
        size = chunk.shape[0]
        full = lambda *_: (0, 0)
        k_of = lambda i: jnp.minimum(i, peers - 1)
        n_of = lambda i: jnp.maximum(i - peers, 0)
        spec = pltpu.PrefetchScalarGridSpec(
            num_scalar_prefetch=1,
            grid=(2 * peers,),
            in_specs=[pl.BlockSpec((size, width), full)] * peers
            + [
                pl.BlockSpec((padded_peers, width), full),
                pl.BlockSpec((None, width, hidden_units), lambda i, h: (0, h[1] ^ k_of(i), 0)),
                pl.BlockSpec((None, width, hidden_units), lambda i, h: (0, h[1] ^ k_of(i), 0)),
                pl.BlockSpec((None, hidden_units, width), lambda i, h: (0, 0, h[1] ^ n_of(i))),
            ],
            out_specs=[pl.BlockSpec((size, width), full)] * peers,
            scratch_shapes=[
                pltpu.VMEM((size, hidden_units), F32),
                pltpu.VMEM((size, hidden_units), F32),
                pltpu.VMEM((size, LANES), F32),
                pltpu.VMEM((size, hidden_units), BF16),
            ],
        )
        parts = pl.pallas_call(
            functools.partial(ffn_kernel, peers=peers),
            grid_spec=spec,
            out_shape=[jax.ShapeDtypeStruct((size, width), BF16)] * peers,
            name="ffn",
        )(here, *blocks, inverse, expert_gate, expert_up, expert_down)
        total = parts[0].astype(F32)
        for k in range(1, peers):
            total = total + swap(parts[k], "tp", k).astype(F32)
        return total.astype(BF16)

    half = spots // 2
    near = expert(jnp.concatenate(arrived[:half], axis=0))
    far = expert(jnp.concatenate(arrived[half:], axis=0))
    back = []
    for d in range(spots):
        source, at = (near, d) if d < half else (far, d - half)
        piece = source[at * capacity : (at + 1) * capacity]
        back.append(piece if d == 0 else swap(piece, "sp", d))

    return pl.pallas_call(
        functools.partial(combine_kernel, spots=spots, topk=topk),
        out_shape=jax.ShapeDtypeStruct((rows, width), BF16),
        in_specs=[VMEM_SPEC] * (spots + 3),
        out_specs=VMEM_SPEC,
        name="combine",
    )(*back, slots_col, route_weight, mixed)


def solution(mesh):
    in_specs = (
        P("sp", "tp"),
        P("sp", "tp"),
        P("sp", "tp"),
        P(None, "tp"),
        P("tp"),
        P("tp"),
        P("tp"),
        P(None, "tp"),
        P("tp"),
        P("sp", None),
        P("sp", None),
        P("sp", None, "tp"),
        P("sp", None, "tp"),
        P("sp", "tp", None),
    )
    out_specs = P("sp", "tp")
    return jax.shard_map(
        on_device, mesh=mesh, in_specs=in_specs, out_specs=out_specs, check_vma=False
    )
```

time: 185 us -> 118 us (0.64)
  blocking collectives: 51.5 us -> 0 us
  waiting for transfers between devices: 83.6 us -> 34.5 us
  Pallas kernels: 0 us -> 34.8 us
  starting transfers between devices: 8.34 us -> 37.1 us
  matrix products: 18.2 us -> 0 us
  between operations: 13.6 us -> 0.26 us
  local copies, waits for them, and re-layouts: 3.76 us -> 7.81 us
  other arithmetic: 5.59 us -> 2.89 us
    reduce_scatter x1 -> x0, waiting for transfers between devices: 35.3 us -> none  [on_device(): lax.psum_scatter(partial_out.astype(jnp.bfloat16), 'tp', scatter_dimensio...]
    pallas_call x0 -> x6, Pallas kernels: none -> 34.8 us  [the longest x2 23.5 us: expert(): pl.pallas_call(functools.partial(ffn_kernel, peers=peers), grid_spec=spec...]
    ppermute x2 -> x31, waiting for transfers between devices: 0.01 us -> 34.5 us  [the longest x29 30.6 us: swap(): return lax.ppermute(value, axis, [(i, i ^ offset) for i in range(count)])]
    ppermute x2 -> x31, starting transfers between devices: 3.69 us -> 37.1 us  [the longest x29 33.5 us: swap(): return lax.ppermute(value, axis, [(i, i ^ offset) for i in range(count)])]
    all_gather x1 -> x0, waiting for transfers between devices: 33.1 us -> none  [on_device(): lax.all_gather(arrived.reshape(experts * capacity, normed.shape[1]), 'tp'...]
    all_to_all x1 -> x0, blocking collectives: 22.2 us -> none  [on_device(): lax.all_to_all(outgoing, 'sp', split_axis=0, concat_axis=0, tiled=True)]
    psum x2 -> x0, blocking collectives: 19.7 us -> none  [the longest x1 10.7 us: on_device(): lax.psum((jnp.sum(conv, axis=1), jnp.sum(conv * conv, axis=1)), 'tp')]
    dot_general x5 -> x0, matrix products: 18.2 us -> none  [the longest x1 10.5 us: on_device(): jnp.dot(hidden, expert_down[0], preferred_element_type=jnp.float32)]
  transfers between devices with their start and end apart: 5 -> 31, of which waited for: 3 -> 13; matrix products, arithmetic and copies ran while one was open for 2% -> 5% of each run, Pallas kernels for 0% -> 22%
where the time goes in v1:
time: 118 us; the launch traced here: 117 us
  starting transfers between devices  37.1 us (31%)
  Pallas kernels  34.8 us (29%)
  waiting for transfers between devices  34.5 us (29%)
  local copies, waits for them, and re-layouts  7.81 us (7%)
  other arithmetic  2.89 us (2%)
    ppermute x29, starting transfers between devices, swap(): return lax.ppermute(value, axis, [(i, i ^ offset) for i in range(count)])  33.5 us
    ppermute x29, waiting for transfers between devices, swap(): return lax.ppermute(value, axis, [(i, i ^ offset) for i in range(count)])  30.6 us
    pallas_call x2, Pallas kernels, expert(): pl.pallas_call(functools.partial(ffn_kernel, peers=peers), grid_spec=spec...  23.5 us
    unnamed x54, local copies, waits for them, and re-layouts  7.12 us
    ppermute x1, waiting for transfers between devices, on_device(): after = lax.ppermute(gated[:edge], 'sp', [(i + 1, i) for i in range(ends)])  3.94 us
    pallas_call x1, Pallas kernels, on_device(): pl.pallas_call(functools.partial(mix_kernel, peers=peers, spots=spots, ca...  3.88 us
    pallas_call x1, Pallas kernels, on_device(): pl.pallas_call(conv_kernel, out_shape=jax.ShapeDtypeStruct((rows + SUB, w...  3.05 us
    ppermute x1, starting transfers between devices, on_device(): lax.ppermute(gated[rows - edge:], 'sp', [(i, i + 1) for i in range(ends)])  2.4 us
  transfers between devices with their start and end apart: 31, of which 13 were waited for; matrix products, arithmetic and copies ran while one was open for 5% of the time, Pallas kernels for 22%

profile of v1, /device:TPU:0, one launch (start us, length us, event | category | flops | bytes accessed | tf_op | source)
XLA Modules:
  0.0 117.4 jit_solution(8360094481713873970)
XLA Ops:
  0.0 1.0 multiply_convert_fusion.gated
  1.1 2.4 %collective-permute-start = (bf16[16,512]{1,0:T(8,128)(2,1)S(1)}, bf16[16,512]{1,0:T(8,128)(2,1)S(1)}, u32[]{:S(2)}, u32[]{:S(2)}) collective-permute-start(bf16[16,512]{1,0:T(8,128)(2,1)S(1)} %get-tuple-element.54), channel_id=1, source_target_pairs={{0,4},{4,8},{8,12},{12,16},{16,20},{20,24},{24,28},{1,5},{5,9},{9,... | collective-permute-start | bytes 49160 | tf_op jit(solution)/shard_map/ppermute | solution.py:239
  3.5 1.3 %collective-permute-start.1 = (bf16[16,512]{1,0:T(8,128)(2,1)S(1)}, bf16[16,512]{1,0:T(8,128)(2,1)S(1)}, u32[]{:S(2)}, u32[]{:S(2)}) collective-permute-start(bf16[16,512]{1,0:T(8,128)(2,1)S(1)} %get-tuple-element.53), channel_id=1, source_target_pairs={{4,0},{8,4},{12,8},{16,12},{20,16},{24,20},{28,24},{5,1},{9,5},{13... | collective-permute-start | bytes 49160 | tf_op jit(solution)/shard_map/ppermute | solution.py:240
  4.8 3.9 %collective-permute-done.1.after = bf16[16,512]{1,0:T(8,128)(2,1)S(1)} collective-permute-done((bf16[16,512]{1,0:T(8,128)(2,1)S(1)}, bf16[16,512]{1,0:T(8,128)(2,1)S(1)}, u32[]{:S(2)}, u32[]{:S(2)}) %collective-permute-start.1) | collective-permute-done | bytes 16416 | tf_op jit(solution)/shard_map/ppermute | solution.py:240
  9.3 3.1 %conv.1.refs_0_ = bf16[144,512]{1,0:T(8,128)(2,1)} custom-call(bf16[16,512]{1,0:T(8,128)(2,1)} %copy-done.20, bf16[128,512]{1,0:T(8,128)(2,1)} %copy-done, bf16[16,512]{1,0:T(8,128)(2,1)} %copy-done.21, bf16[31,512]{1,0:T(8,128)(2,1)} %taps.1, f32[1,512]{1,0:T(1,128)} %bitcast.6, f32[1,512]{1,0:T(1,128)} %bitcast.7, f32[1,512]{1,0:T(1,128)} %bitcast.8, ...), custom_call_target="tpu_custom_call" | custom-call | tf_op jit(solution)/shard_map/conv/pallas_call | solution.py:253
  12.4 1.5 %collective-permute-start.2 = (bf16[144,512]{1,0:T(8,128)(2,1)}, bf16[144,512]{1,0:T(8,128)(2,1)S(1)}, u32[]{:S(2)}, u32[]{:S(2)}) collective-permute-start(bf16[144,512]{1,0:T(8,128)(2,1)} %conv.1.refs_0_), channel_id=1, source_target_pairs={{0,1},{1,0},{2,3},{3,2},{4,5},{5,4},{6,7},{7,6},{8,9},{9,8},{10,11... | collective-permute-start | bytes 442376 | tf_op jit(solution)/shard_map/ppermute | solution.py:20
  13.9 1.5 %collective-permute-start.3 = (bf16[144,512]{1,0:T(8,128)(2,1)}, bf16[144,512]{1,0:T(8,128)(2,1)S(1)}, u32[]{:S(2)}, u32[]{:S(2)}) collective-permute-start(bf16[144,512]{1,0:T(8,128)(2,1)} %conv.1.refs_0_), channel_id=1, source_target_pairs={{0,2},{1,3},{2,0},{3,1},{4,6},{5,7},{6,4},{7,5},{8,10},{9,11},{10,... | collective-permute-start | bytes 442376 | tf_op jit(solution)/shard_map/ppermute | solution.py:20
  15.9 1.4 %copy.15.ids = s32[128,2]{1,0:T(8,128)} copy(s32[128,2]{0,1:T(2,128)} %param.23) | data formatting | bytes 2048 | tf_op args[9]
  17.3 0.6 pad_add_fusion.here
  17.9 2.0 %route.1 = (s32[128,128]{1,0:T(8,128)}, s32[8,128]{1,0:T(8,128)}) custom-call(s32[2]{0:T(128)} %pad_add_fusion.here, s32[128,2]{1,0:T(8,128)} %copy.15.ids), custom_call_target="tpu_custom_call" | custom-call | tf_op jit(solution)/shard_map/route/pallas_call | solution.py:242
  19.9 2.9 %collective-permute-done.4.refs_3_ = bf16[144,512]{1,0:T(8,128)(2,1)S(1)} collective-permute-done((bf16[144,512]{1,0:T(8,128)(2,1)}, bf16[144,512]{1,0:T(8,128)(2,1)S(1)}, u32[]{:S(2)}, u32[]{:S(2)}) %collective-permute-start.4) | collective-permute-done | bytes 147488 | tf_op jit(solution)/shard_map/ppermute | solution.py:20
  22.8 0.7 copy-done.12
  23.5 3.9 %mix.1 = (f32[128,512]{1,0:T(8,128)}, f32[8,512]{1,0:T(8,128)}, bf16[64,512]{1,0:T(8,128)(2,1)}, bf16[64,512]{1,0:T(8,128)(2,1)}, bf16[64,512]{1,0:T(8,128)(2,1)...) custom-call(s32[2]{0:T(128)} %pad_add_fusion.here, ...), custom_call_target="tpu_custom_call" | custom-call | tf_op jit(solution)/shard_map/mix/pallas_call | solution.py:273
  27.4 4.2 %collective-permute-start.17 = (bf16[64,512]{1,0:T(8,128)(2,1)}, bf16[64,512]{1,0:T(8,128)(2,1)S(1)}, u32[]{:S(2)}, u32[]{:S(2)}) collective-permute-start(bf16[64,512]{1,0:T(8,128)(2,1)} %get-tuple-element.35), channel_id=1, source_target_pairs={{0,16},{4,20},{8,24},{12,28},{16,0},{20,4},{24,8},{28,12},{1,17},{... | collective-permute-start | bytes 196616 | tf_op jit(solution)/shard_map/ppermute | solution.py:20
  31.6 1.3 %collective-permute-start.19 = (bf16[64,512]{1,0:T(8,128)(2,1)}, bf16[64,512]{1,0:T(8,128)(2,1)S(1)}, u32[]{:S(2)}, u32[]{:S(2)}) collective-permute-start(bf16[64,512]{1,0:T(8,128)(2,1)} %get-tuple-element.37), channel_id=1, source_target_pairs={{0,24},{4,28},{8,16},{12,20},{16,8},{20,12},{24,0},{28,4},{1,25},{... | collective-permute-start | bytes 196616 | tf_op jit(solution)/shard_map/ppermute | solution.py:20
  32.9 2.0 %collective-permute-start.20 = (bf16[64,512]{1,0:T(8,128)(2,1)}, bf16[64,512]{1,0:T(8,128)(2,1)S(1)}, u32[]{:S(2)}, u32[]{:S(2)}) collective-permute-start(bf16[64,512]{1,0:T(8,128)(2,1)} %get-tuple-element.38), channel_id=1, source_target_pairs={{0,28},{4,24},{8,20},{12,16},{16,12},{20,8},{24,4},{28,0},{1,29},{... | collective-permute-start | bytes 196616 | tf_op jit(solution)/shard_map/ppermute | solution.py:20
  35.5 0.8 constant_dynamic-update-slice_fusion.3
  36.4 3.9 %collective-permute-done.17 = bf16[64,512]{1,0:T(8,128)(2,1)S(1)} collective-permute-done((bf16[64,512]{1,0:T(8,128)(2,1)}, bf16[64,512]{1,0:T(8,128)(2,1)S(1)}, u32[]{:S(2)}, u32[]{:S(2)}) %collective-permute-start.17) | collective-permute-done | bytes 65568 | tf_op jit(solution)/shard_map/ppermute | solution.py:20
  40.3 0.9 collective-permute-done.18
  41.2 1.0 collective-permute-start.21
  42.2 1.2 collective-permute-start.22
  43.4 1.4 %collective-permute-start.23 = (bf16[256,512]{1,0:T(8,128)(2,1)S(1)}, bf16[256,512]{1,0:T(8,128)(2,1)S(1)}, u32[]{:S(2)}, u32[]{:S(2)}) collective-permute-start(bf16[256,512]{1,0:T(8,128)(2,1)S(1)} %constant_dynamic-update-slice_fusion.4.refs_0_), channel_id=1, source_target_pairs={{0,3},{1,2},{2,1},{3,0},{4,7},{5,6},{6,5},{7,4},{8,11},{9,10},{10,... | collective-permute-start | bytes 786440 | tf_op jit(solution)/shard_map/ppermute | solution.py:20
  45.1 0.7 collective-permute-done.7
  45.8 1.6 %collective-permute-start.10 = (bf16[256,512]{1,0:T(8,128)(2,1)S(1)}, bf16[256,512]{1,0:T(8,128)(2,1)S(1)}, u32[]{:S(2)}, u32[]{:S(2)}) collective-permute-start(bf16[256,512]{1,0:T(8,128)(2,1)S(1)} %constant_dynamic-update-slice_fusion.refs_0_), channel_id=1, source_target_pairs={{0,3},{1,2},{2,1},{3,0},{4,7},{5,6},{6,5},{7,4},{8,11},{9,10},{10,... | collective-permute-start | bytes 786440 | tf_op jit(solution)/shard_map/ppermute | solution.py:20
  47.3 1.5 %collective-permute-start.8 = (bf16[256,512]{1,0:T(8,128)(2,1)S(1)}, bf16[256,512]{1,0:T(8,128)(2,1)S(1)}, u32[]{:S(2)}, u32[]{:S(2)}) collective-permute-start(bf16[256,512]{1,0:T(8,128)(2,1)S(1)} %constant_dynamic-update-slice_fusion.refs_0_), channel_id=1, source_target_pairs={{0,1},{1,0},{2,3},{3,2},{4,5},{5,4},{6,7},{7,6},{8,9},{9,8},{10,11... | collective-permute-start | bytes 786440 | tf_op jit(solution)/shard_map/ppermute | solution.py:20
  48.8 1.3 %collective-permute-done.21.refs_1_ = bf16[256,512]{1,0:T(8,128)(2,1)S(1)} collective-permute-done((bf16[256,512]{1,0:T(8,128)(2,1)S(1)}, bf16[256,512]{1,0:T(8,128)(2,1)S(1)}, u32[]{:S(2)}, u32[]{:S(2)}) %collective-permute-start.21) | collective-permute-done | bytes 262176 | tf_op jit(solution)/shard_map/ppermute | solution.py:20
  50.2 1.5 %collective-permute-start.9 = (bf16[256,512]{1,0:T(8,128)(2,1)S(1)}, bf16[256,512]{1,0:T(8,128)(2,1)S(1)}, u32[]{:S(2)}, u32[]{:S(2)}) collective-permute-start(bf16[256,512]{1,0:T(8,128)(2,1)S(1)} %constant_dynamic-update-slice_fusion.refs_0_), channel_id=1, source_target_pairs={{0,2},{1,3},{2,0},{3,1},{4,6},{5,7},{6,4},{7,5},{8,10},{9,11},{10,... | collective-permute-start | bytes 786440 | tf_op jit(solution)/shard_map/ppermute | solution.py:20
  51.7 9.3 %collective-permute-done.22.refs_2_ = bf16[256,512]{1,0:T(8,128)(2,1)S(1)} collective-permute-done((bf16[256,512]{1,0:T(8,128)(2,1)S(1)}, bf16[256,512]{1,0:T(8,128)(2,1)S(1)}, u32[]{:S(2)}, u32[]{:S(2)}) %collective-permute-start.22) | collective-permute-done | bytes 262176 | tf_op jit(solution)/shard_map/ppermute | solution.py:20
  61.0 0.7 copy-done.6
  61.8 11.8 %ffn.3 = (bf16[256,512]{1,0:T(8,128)(2,1)}, bf16[256,512]{1,0:T(8,128)(2,1)}, bf16[256,512]{1,0:T(8,128)(2,1)}, bf16[256,512]{1,0:T(8,128)(2,1)}) custom-call(s32[2]{0:T(128)} %pad_add_fusion.here, bf16[256,512]{1,0:T(8,128)(2,1)} %copy-done.2, bf16[256,512]{1,0:T(8,128)(2,1)} %copy-done.4, bf16[256,512]{1,0:T(8,128)(2,1)} %copy-done.6, ...), custom_call_target="tpu_custom_call" | custom-call | tf_op jit(solution)/shard_map/ffn/pallas_call | solution.py:313
  73.6 2.8 %collective-permute-start.24 = (bf16[256,512]{1,0:T(8,128)(2,1)}, bf16[256,512]{1,0:T(8,128)(2,1)S(1)}, u32[]{:S(2)}, u32[]{:S(2)}) collective-permute-start(bf16[256,512]{1,0:T(8,128)(2,1)} %get-tuple-element.40), channel_id=1, source_target_pairs={{0,1},{1,0},{2,3},{3,2},{4,5},{5,4},{6,7},{7,6},{8,9},{9,8},{10,11... | collective-permute-start | bytes 786440 | tf_op jit(solution)/shard_map/ppermute | solution.py:20
  76.4 1.5 %collective-permute-start.25 = (bf16[256,512]{1,0:T(8,128)(2,1)}, bf16[256,512]{1,0:T(8,128)(2,1)S(1)}, u32[]{:S(2)}, u32[]{:S(2)}) collective-permute-start(bf16[256,512]{1,0:T(8,128)(2,1)} %get-tuple-element.41), channel_id=1, source_target_pairs={{0,2},{1,3},{2,0},{3,1},{4,6},{5,7},{6,4},{7,5},{8,10},{9,11},{10,... | collective-permute-start | bytes 786440 | tf_op jit(solution)/shard_map/ppermute | solution.py:20
  78.8 0.7 copy-done.9
  79.5 11.7 %ffn.2 = (bf16[256,512]{1,0:T(8,128)(2,1)}, bf16[256,512]{1,0:T(8,128)(2,1)}, bf16[256,512]{1,0:T(8,128)(2,1)}, bf16[256,512]{1,0:T(8,128)(2,1)}) custom-call(s32[2]{0:T(128)} %pad_add_fusion.here, bf16[256,512]{1,0:T(8,128)(2,1)} %copy-done.1, bf16[256,512]{1,0:T(8,128)(2,1)} %copy-done.7, bf16[256,512]{1,0:T(8,128)(2,1)} %copy-done.9, ...), custom_call_target="tpu_custom_call" | custom-call | tf_op jit(solution)/shard_map/ffn/pallas_call | solution.py:313
  91.2 1.9 %collective-permute-start.11 = (bf16[256,512]{1,0:T(8,128)(2,1)}, bf16[256,512]{1,0:T(8,128)(2,1)S(1)}, u32[]{:S(2)}, u32[]{:S(2)}) collective-permute-start(bf16[256,512]{1,0:T(8,128)(2,1)} %get-tuple-element.32), channel_id=1, source_target_pairs={{0,1},{1,0},{2,3},{3,2},{4,5},{5,4},{6,7},{7,6},{8,9},{9,8},{10,11... | collective-permute-start | bytes 786440 | tf_op jit(solution)/shard_map/ppermute | solution.py:20
  93.1 1.5 %collective-permute-start.12 = (bf16[256,512]{1,0:T(8,128)(2,1)}, bf16[256,512]{1,0:T(8,128)(2,1)S(1)}, u32[]{:S(2)}, u32[]{:S(2)}) collective-permute-start(bf16[256,512]{1,0:T(8,128)(2,1)} %get-tuple-element.33), channel_id=1, source_target_pairs={{0,2},{1,3},{2,0},{3,1},{4,6},{5,7},{6,4},{7,5},{8,10},{9,11},{10,... | collective-permute-start | bytes 786440 | tf_op jit(solution)/shard_map/ppermute | solution.py:20
  94.8 3.9 %collective-permute-start.27 = (bf16[64,512]{1,0:T(8,128)(2,1)S(1)}, bf16[64,512]{1,0:T(8,128)(2,1)S(1)}, u32[]{:S(2)}, u32[]{:S(2)}) collective-permute-start(bf16[64,512]{1,0:T(8,128)(2,1)S(1)} %get-tuple-element.48), channel_id=1, source_target_pairs={{0,16},{4,20},{8,24},{12,28},{16,0},{20,4},{24,8},{28,12},{1,17},{... | collective-permute-start | bytes 196616 | tf_op jit(solution)/shard_map/ppermute | solution.py:20
  98.8 1.8 %collective-permute-done.11 = bf16[256,512]{1,0:T(8,128)(2,1)S(1)} collective-permute-done((bf16[256,512]{1,0:T(8,128)(2,1)}, bf16[256,512]{1,0:T(8,128)(2,1)S(1)}, u32[]{:S(2)}, u32[]{:S(2)}) %collective-permute-start.11) | collective-permute-done | bytes 262176 | tf_op jit(solution)/shard_map/ppermute | solution.py:20
  100.6 5.7 %collective-permute-done.12 = bf16[256,512]{1,0:T(8,128)(2,1)S(1)} collective-permute-done((bf16[256,512]{1,0:T(8,128)(2,1)}, bf16[256,512]{1,0:T(8,128)(2,1)S(1)}, u32[]{:S(2)}, u32[]{:S(2)}) %collective-permute-start.12) | collective-permute-done | bytes 262176 | tf_op jit(solution)/shard_map/ppermute | solution.py:20
  106.2 1.1 add_convert_fusion.1
  107.3 0.6 fusion.1
  108.0 0.6 collective-permute-start.15
  108.6 1.2 %collective-permute-start.16 = (bf16[64,512]{1,0:T(8,128)(2,1)S(1)}, bf16[64,512]{1,0:T(8,128)(2,1)S(1)}, u32[]{:S(2)}, u32[]{:S(2)}) collective-permute-start(bf16[64,512]{1,0:T(8,128)(2,1)S(1)} %get-tuple-element.49), channel_id=1, source_target_pairs={{0,12},{4,8},{8,4},{12,0},{16,28},{20,24},{24,20},{28,16},{1,13},{... | collective-permute-start | bytes 196616 | tf_op jit(solution)/shard_map/ppermute | solution.py:20
  109.8 0.7 copy.16.refs_9_
  110.6 1.2 %collective-permute-done.30.refs_7_ = bf16[64,512]{1,0:T(8,128)(2,1)S(1)} collective-permute-done((bf16[64,512]{1,0:T(8,128)(2,1)S(1)}, bf16[64,512]{1,0:T(8,128)(2,1)S(1)}, u32[]{:S(2)}, u32[]{:S(2)}) %collective-permute-start.30) | collective-permute-done | bytes 65568 | tf_op jit(solution)/shard_map/ppermute | solution.py:20
  111.8 1.4 %collective-permute-done.15.refs_2_ = bf16[64,512]{1,0:T(8,128)(2,1)S(1)} collective-permute-done((bf16[64,512]{1,0:T(8,128)(2,1)S(1)}, bf16[64,512]{1,0:T(8,128)(2,1)S(1)}, u32[]{:S(2)}, u32[]{:S(2)}) %collective-permute-start.15) | collective-permute-done | bytes 65568 | tf_op jit(solution)/shard_map/ppermute | solution.py:20
  113.1 1.3 %collective-permute-done.16.refs_3_ = bf16[64,512]{1,0:T(8,128)(2,1)S(1)} collective-permute-done((bf16[64,512]{1,0:T(8,128)(2,1)S(1)}, bf16[64,512]{1,0:T(8,128)(2,1)S(1)}, u32[]{:S(2)}, u32[]{:S(2)}) %collective-permute-start.16) | collective-permute-done | bytes 65568 | tf_op jit(solution)/shard_map/ppermute | solution.py:20
  115.1 2.3 %combine.1 = bf16[128,512]{1,0:T(8,128)(2,1)} custom-call(bf16[64,512]{1,0:T(8,128)(2,1)} %get-tuple-element.52.refs_0_, bf16[64,512]{1,0:T(8,128)(2,1)} %copy-done.17, bf16[64,512]{1,0:T(8,128)(2,1)} %copy-done.18, bf16[64,512]{1,0:T(8,128)(2,1)} %copy-done.19, bf16[64,512]{1,0:T(8,128)(2,1)} %copy-done.13, bf16[64,512]{1,0:T(8,128)(2,1)} %copy-done.14, ...), custom_call_target="tpu_custom_call" | custom-call | tf_op jit(solution)/shard_map/combine/pallas_call | solution.py:333
  (83 shorter events, 3.7 us)
Async XLA Ops:
  1.0 7.7 %copy-start = (bf16[128,512]{1,0:T(8,128)(2,1)}, bf16[128,512]{1,0:T(8,128)(2,1)S(1)}, u32[]{:S(2)}) copy-start(bf16[128,512]{1,0:T(8,128)(2,1)S(1)} %multiply_convert_fusion.gated) | copy-start | bytes 393220
  1.1 3.7 %collective-permute-start = (bf16[16,512]{1,0:T(8,128)(2,1)S(1)}, bf16[16,512]{1,0:T(8,128)(2,1)S(1)}, u32[]{:S(2)}, u32[]{:S(2)}) collective-permute-start(bf16[16,512]{1,0:T(8,128)(2,1)S(1)} %get-tuple-element.54), channel_id=1, source_target_pairs={{0,4},{4,8},{8,12},{12,16},{16,20},{20,24},{24,28},{1,5},{5,9},{9,... | collective-permute-start | bytes 49160 | tf_op jit(solution)/shard_map/ppermute | solution.py:239
  3.5 5.3 %collective-permute-start.1 = (bf16[16,512]{1,0:T(8,128)(2,1)S(1)}, bf16[16,512]{1,0:T(8,128)(2,1)S(1)}, u32[]{:S(2)}, u32[]{:S(2)}) collective-permute-start(bf16[16,512]{1,0:T(8,128)(2,1)S(1)} %get-tuple-element.53), channel_id=1, source_target_pairs={{4,0},{8,4},{12,8},{16,12},{20,16},{24,20},{28,24},{5,1},{9,5},{13... | collective-permute-start | bytes 49160 | tf_op jit(solution)/shard_map/ppermute | solution.py:240
  4.8 4.0 %copy-start.20 = (bf16[16,512]{1,0:T(8,128)(2,1)}, bf16[16,512]{1,0:T(8,128)(2,1)S(1)}, u32[]{:S(2)}) copy-start(bf16[16,512]{1,0:T(8,128)(2,1)S(1)} %collective-permute-done.before) | copy-start | bytes 49156
  12.4 7.5 %collective-permute-start.2 = (bf16[144,512]{1,0:T(8,128)(2,1)}, bf16[144,512]{1,0:T(8,128)(2,1)S(1)}, u32[]{:S(2)}, u32[]{:S(2)}) collective-permute-start(bf16[144,512]{1,0:T(8,128)(2,1)} %conv.1.refs_0_), channel_id=1, source_target_pairs={{0,1},{1,0},{2,3},{3,2},{4,5},{5,4},{6,7},{7,6},{8,9},{9,8},{10,11... | collective-permute-start | bytes 442376 | tf_op jit(solution)/shard_map/ppermute | solution.py:20
  13.9 6.0 %collective-permute-start.3 = (bf16[144,512]{1,0:T(8,128)(2,1)}, bf16[144,512]{1,0:T(8,128)(2,1)S(1)}, u32[]{:S(2)}, u32[]{:S(2)}) collective-permute-start(bf16[144,512]{1,0:T(8,128)(2,1)} %conv.1.refs_0_), channel_id=1, source_target_pairs={{0,2},{1,3},{2,0},{3,1},{4,6},{5,7},{6,4},{7,5},{8,10},{9,11},{10,... | collective-permute-start | bytes 442376 | tf_op jit(solution)/shard_map/ppermute | solution.py:20
  15.4 7.4 %collective-permute-start.4 = (bf16[144,512]{1,0:T(8,128)(2,1)}, bf16[144,512]{1,0:T(8,128)(2,1)S(1)}, u32[]{:S(2)}, u32[]{:S(2)}) collective-permute-start(bf16[144,512]{1,0:T(8,128)(2,1)} %conv.1.refs_0_), channel_id=1, source_target_pairs={{0,3},{1,2},{2,1},{3,0},{4,7},{5,6},{6,5},{7,4},{8,11},{9,10},{10,... | collective-permute-start | bytes 442376 | tf_op jit(solution)/shard_map/ppermute | solution.py:20
  19.9 2.9 %copy-start.10 = (bf16[144,512]{1,0:T(8,128)(2,1)}, bf16[144,512]{1,0:T(8,128)(2,1)S(1)}, u32[]{:S(2)}) copy-start(bf16[144,512]{1,0:T(8,128)(2,1)S(1)} %collective-permute-done.2.refs_1_) | copy-start | bytes 442372
  19.9 2.9 %copy-start.11 = (bf16[144,512]{1,0:T(8,128)(2,1)}, bf16[144,512]{1,0:T(8,128)(2,1)S(1)}, u32[]{:S(2)}) copy-start(bf16[144,512]{1,0:T(8,128)(2,1)S(1)} %collective-permute-done.3.refs_2_) | copy-start | bytes 442372
  27.4 12.9 %collective-permute-start.17 = (bf16[64,512]{1,0:T(8,128)(2,1)}, bf16[64,512]{1,0:T(8,128)(2,1)S(1)}, u32[]{:S(2)}, u32[]{:S(2)}) collective-permute-start(bf16[64,512]{1,0:T(8,128)(2,1)} %get-tuple-element.35), channel_id=1, source_target_pairs={{0,16},{4,20},{8,24},{12,28},{16,0},{20,4},{24,8},{28,12},{1,17},{... | collective-permute-start | bytes 196616 | tf_op jit(solution)/shard_map/ppermute | solution.py:20
  31.6 9.6 %collective-permute-start.18 = (bf16[64,512]{1,0:T(8,128)(2,1)}, bf16[64,512]{1,0:T(8,128)(2,1)S(1)}, u32[]{:S(2)}, u32[]{:S(2)}) collective-permute-start(bf16[64,512]{1,0:T(8,128)(2,1)} %get-tuple-element.36), channel_id=1, source_target_pairs={{0,20},{4,16},{8,28},{12,24},{16,4},{20,0},{24,12},{28,8},{1,21},{... | collective-permute-start | bytes 196616 | tf_op jit(solution)/shard_map/ppermute | solution.py:20
  31.6 9.6 %collective-permute-start.19 = (bf16[64,512]{1,0:T(8,128)(2,1)}, bf16[64,512]{1,0:T(8,128)(2,1)S(1)}, u32[]{:S(2)}, u32[]{:S(2)}) collective-permute-start(bf16[64,512]{1,0:T(8,128)(2,1)} %get-tuple-element.37), channel_id=1, source_target_pairs={{0,24},{4,28},{8,16},{12,20},{16,8},{20,12},{24,0},{28,4},{1,25},{... | collective-permute-start | bytes 196616 | tf_op jit(solution)/shard_map/ppermute | solution.py:20
  32.9 8.3 %collective-permute-start.20 = (bf16[64,512]{1,0:T(8,128)(2,1)}, bf16[64,512]{1,0:T(8,128)(2,1)S(1)}, u32[]{:S(2)}, u32[]{:S(2)}) collective-permute-start(bf16[64,512]{1,0:T(8,128)(2,1)} %get-tuple-element.38), channel_id=1, source_target_pairs={{0,28},{4,24},{8,20},{12,16},{16,12},{20,8},{24,4},{28,0},{1,29},{... | collective-permute-start | bytes 196616 | tf_op jit(solution)/shard_map/ppermute | solution.py:20
  34.9 8.4 %collective-permute-start.5 = (bf16[64,512]{1,0:T(8,128)(2,1)}, bf16[64,512]{1,0:T(8,128)(2,1)S(1)}, u32[]{:S(2)}, u32[]{:S(2)}) collective-permute-start(bf16[64,512]{1,0:T(8,128)(2,1)} %get-tuple-element.27), channel_id=1, source_target_pairs={{0,4},{4,0},{8,12},{12,8},{16,20},{20,16},{24,28},{28,24},{1,5},{5... | collective-permute-start | bytes 196616 | tf_op jit(solution)/shard_map/ppermute | solution.py:20
  40.2 4.8 %collective-permute-start.6 = (bf16[64,512]{1,0:T(8,128)(2,1)}, bf16[64,512]{1,0:T(8,128)(2,1)S(1)}, u32[]{:S(2)}, u32[]{:S(2)}) collective-permute-start(bf16[64,512]{1,0:T(8,128)(2,1)} %get-tuple-element.28), channel_id=1, source_target_pairs={{0,8},{4,12},{8,0},{12,4},{16,24},{20,28},{24,16},{28,20},{1,9},{5... | collective-permute-start | bytes 196616 | tf_op jit(solution)/shard_map/ppermute | solution.py:20
  41.2 4.6 %collective-permute-start.7 = (bf16[64,512]{1,0:T(8,128)(2,1)}, bf16[64,512]{1,0:T(8,128)(2,1)S(1)}, u32[]{:S(2)}, u32[]{:S(2)}) collective-permute-start(bf16[64,512]{1,0:T(8,128)(2,1)} %get-tuple-element.29), channel_id=1, source_target_pairs={{0,12},{4,8},{8,4},{12,0},{16,28},{20,24},{24,20},{28,16},{1,13},{... | collective-permute-start | bytes 196616 | tf_op jit(solution)/shard_map/ppermute | solution.py:20
  41.2 19.7 %copy-start.2 = (bf16[256,512]{1,0:T(8,128)(2,1)}, bf16[256,512]{1,0:T(8,128)(2,1)S(1)}, u32[]{:S(2)}) copy-start(bf16[256,512]{1,0:T(8,128)(2,1)S(1)} %constant_dynamic-update-slice_fusion.4.refs_0_) | copy-start | bytes 786436
  41.2 8.9 %collective-permute-start.21 = (bf16[256,512]{1,0:T(8,128)(2,1)S(1)}, bf16[256,512]{1,0:T(8,128)(2,1)S(1)}, u32[]{:S(2)}, u32[]{:S(2)}) collective-permute-start(bf16[256,512]{1,0:T(8,128)(2,1)S(1)} %constant_dynamic-update-slice_fusion.4.refs_0_), channel_id=1, source_target_pairs={{0,1},{1,0},{2,3},{3,2},{4,5},{5,4},{6,7},{7,6},{8,9},{9,8},{10,11... | collective-permute-start | bytes 786440 | tf_op jit(solution)/shard_map/ppermute | solution.py:20
  42.2 18.8 %collective-permute-start.22 = (bf16[256,512]{1,0:T(8,128)(2,1)S(1)}, bf16[256,512]{1,0:T(8,128)(2,1)S(1)}, u32[]{:S(2)}, u32[]{:S(2)}) collective-permute-start(bf16[256,512]{1,0:T(8,128)(2,1)S(1)} %constant_dynamic-update-slice_fusion.4.refs_0_), channel_id=1, source_target_pairs={{0,2},{1,3},{2,0},{3,1},{4,6},{5,7},{6,4},{7,5},{8,10},{9,11},{10,... | collective-permute-start | bytes 786440 | tf_op jit(solution)/shard_map/ppermute | solution.py:20
  43.4 17.6 %collective-permute-start.23 = (bf16[256,512]{1,0:T(8,128)(2,1)S(1)}, bf16[256,512]{1,0:T(8,128)(2,1)S(1)}, u32[]{:S(2)}, u32[]{:S(2)}) collective-permute-start(bf16[256,512]{1,0:T(8,128)(2,1)S(1)} %constant_dynamic-update-slice_fusion.4.refs_0_), channel_id=1, source_target_pairs={{0,3},{1,2},{2,1},{3,0},{4,7},{5,6},{6,5},{7,4},{8,11},{9,10},{10,... | collective-permute-start | bytes 786440 | tf_op jit(solution)/shard_map/ppermute | solution.py:20
  45.8 27.9 %copy-start.1 = (bf16[256,512]{1,0:T(8,128)(2,1)}, bf16[256,512]{1,0:T(8,128)(2,1)S(1)}, u32[]{:S(2)}) copy-start(bf16[256,512]{1,0:T(8,128)(2,1)S(1)} %constant_dynamic-update-slice_fusion.refs_0_) | copy-start | bytes 786436
  45.8 32.2 %collective-permute-start.10 = (bf16[256,512]{1,0:T(8,128)(2,1)S(1)}, bf16[256,512]{1,0:T(8,128)(2,1)S(1)}, u32[]{:S(2)}, u32[]{:S(2)}) collective-permute-start(bf16[256,512]{1,0:T(8,128)(2,1)S(1)} %constant_dynamic-update-slice_fusion.refs_0_), channel_id=1, source_target_pairs={{0,3},{1,2},{2,1},{3,0},{4,7},{5,6},{6,5},{7,4},{8,11},{9,10},{10,... | collective-permute-start | bytes 786440 | tf_op jit(solution)/shard_map/ppermute | solution.py:20
  47.3 30.7 %collective-permute-start.8 = (bf16[256,512]{1,0:T(8,128)(2,1)S(1)}, bf16[256,512]{1,0:T(8,128)(2,1)S(1)}, u32[]{:S(2)}, u32[]{:S(2)}) collective-permute-start(bf16[256,512]{1,0:T(8,128)(2,1)S(1)} %constant_dynamic-update-slice_fusion.refs_0_), channel_id=1, source_target_pairs={{0,1},{1,0},{2,3},{3,2},{4,5},{5,4},{6,7},{7,6},{8,9},{9,8},{10,11... | collective-permute-start | bytes 786440 | tf_op jit(solution)/shard_map/ppermute | solution.py:20
  50.2 10.8 %copy-start.4 = (bf16[256,512]{1,0:T(8,128)(2,1)}, bf16[256,512]{1,0:T(8,128)(2,1)S(1)}, u32[]{:S(2)}) copy-start(bf16[256,512]{1,0:T(8,128)(2,1)S(1)} %collective-permute-done.21.refs_1_) | copy-start | bytes 786436
  50.2 27.9 %collective-permute-start.9 = (bf16[256,512]{1,0:T(8,128)(2,1)S(1)}, bf16[256,512]{1,0:T(8,128)(2,1)S(1)}, u32[]{:S(2)}, u32[]{:S(2)}) collective-permute-start(bf16[256,512]{1,0:T(8,128)(2,1)S(1)} %constant_dynamic-update-slice_fusion.refs_0_), channel_id=1, source_target_pairs={{0,2},{1,3},{2,0},{3,1},{4,6},{5,7},{6,4},{7,5},{8,10},{9,11},{10,... | collective-permute-start | bytes 786440 | tf_op jit(solution)/shard_map/ppermute | solution.py:20
  61.0 0.7 copy-start.6
  61.0 0.8 copy-start.8
  73.6 21.0 %collective-permute-start.24 = (bf16[256,512]{1,0:T(8,128)(2,1)}, bf16[256,512]{1,0:T(8,128)(2,1)S(1)}, u32[]{:S(2)}, u32[]{:S(2)}) collective-permute-start(bf16[256,512]{1,0:T(8,128)(2,1)} %get-tuple-element.40), channel_id=1, source_target_pairs={{0,1},{1,0},{2,3},{3,2},{4,5},{5,4},{6,7},{7,6},{8,9},{9,8},{10,11... | collective-permute-start | bytes 786440 | tf_op jit(solution)/shard_map/ppermute | solution.py:20
  76.4 18.3 %collective-permute-start.25 = (bf16[256,512]{1,0:T(8,128)(2,1)}, bf16[256,512]{1,0:T(8,128)(2,1)S(1)}, u32[]{:S(2)}, u32[]{:S(2)}) collective-permute-start(bf16[256,512]{1,0:T(8,128)(2,1)} %get-tuple-element.41), channel_id=1, source_target_pairs={{0,2},{1,3},{2,0},{3,1},{4,6},{5,7},{6,4},{7,5},{8,10},{9,11},{10,... | collective-permute-start | bytes 786440 | tf_op jit(solution)/shard_map/ppermute | solution.py:20
  77.9 16.7 %copy-start.3 = (bf16[256,512]{1,0:T(8,128)(2,1)S(1)}, bf16[256,512]{1,0:T(8,128)(2,1)}, u32[]{:S(2)}) copy-start(bf16[256,512]{1,0:T(8,128)(2,1)} %get-tuple-element.39) | copy-start | bytes 786436
  77.9 31.9 %copy-start.22 = (f32[128,2]{0,1:T(2,128)S(1)}, f32[128,2]{0,1:T(2,128)}, u32[]{:S(2)}) copy-start(f32[128,2]{0,1:T(2,128)} %param.24) | copy-start | bytes 3076
  78.0 16.7 %collective-permute-start.26 = (bf16[256,512]{1,0:T(8,128)(2,1)}, bf16[256,512]{1,0:T(8,128)(2,1)S(1)}, u32[]{:S(2)}, u32[]{:S(2)}) collective-permute-start(bf16[256,512]{1,0:T(8,128)(2,1)} %get-tuple-element.42), channel_id=1, source_target_pairs={{0,3},{1,2},{2,1},{3,0},{4,7},{5,6},{6,5},{7,4},{8,11},{9,10},{10,... | collective-permute-start | bytes 786440 | tf_op jit(solution)/shard_map/ppermute | solution.py:20
  91.2 9.4 %collective-permute-start.11 = (bf16[256,512]{1,0:T(8,128)(2,1)}, bf16[256,512]{1,0:T(8,128)(2,1)S(1)}, u32[]{:S(2)}, u32[]{:S(2)}) collective-permute-start(bf16[256,512]{1,0:T(8,128)(2,1)} %get-tuple-element.32), channel_id=1, source_target_pairs={{0,1},{1,0},{2,3},{3,2},{4,5},{5,4},{6,7},{7,6},{8,9},{9,8},{10,11... | collective-permute-start | bytes 786440 | tf_op jit(solution)/shard_map/ppermute | solution.py:20
  93.1 13.1 %collective-permute-start.12 = (bf16[256,512]{1,0:T(8,128)(2,1)}, bf16[256,512]{1,0:T(8,128)(2,1)S(1)}, u32[]{:S(2)}, u32[]{:S(2)}) collective-permute-start(bf16[256,512]{1,0:T(8,128)(2,1)} %get-tuple-element.33), channel_id=1, source_target_pairs={{0,2},{1,3},{2,0},{3,1},{4,6},{5,7},{6,4},{7,5},{8,10},{9,11},{10,... | collective-permute-start | bytes 786440 | tf_op jit(solution)/shard_map/ppermute | solution.py:20
  94.6 11.6 %collective-permute-start.13 = (bf16[256,512]{1,0:T(8,128)(2,1)}, bf16[256,512]{1,0:T(8,128)(2,1)S(1)}, u32[]{:S(2)}, u32[]{:S(2)}) collective-permute-start(bf16[256,512]{1,0:T(8,128)(2,1)} %get-tuple-element.34), channel_id=1, source_target_pairs={{0,3},{1,2},{2,1},{3,0},{4,7},{5,6},{6,5},{7,4},{8,11},{9,10},{10,... | collective-permute-start | bytes 786440 | tf_op jit(solution)/shard_map/ppermute | solution.py:20
  94.8 13.1 %collective-permute-start.27 = (bf16[64,512]{1,0:T(8,128)(2,1)S(1)}, bf16[64,512]{1,0:T(8,128)(2,1)S(1)}, u32[]{:S(2)}, u32[]{:S(2)}) collective-permute-start(bf16[64,512]{1,0:T(8,128)(2,1)S(1)} %get-tuple-element.48), channel_id=1, source_target_pairs={{0,16},{4,20},{8,24},{12,28},{16,0},{20,4},{24,8},{28,12},{1,17},{... | collective-permute-start | bytes 196616 | tf_op jit(solution)/shard_map/ppermute | solution.py:20
  98.8 9.8 %collective-permute-start.28 = (bf16[64,512]{1,0:T(8,128)(2,1)S(1)}, bf16[64,512]{1,0:T(8,128)(2,1)S(1)}, u32[]{:S(2)}, u32[]{:S(2)}) collective-permute-start(bf16[64,512]{1,0:T(8,128)(2,1)S(1)} %get-tuple-element.47), channel_id=1, source_target_pairs={{0,20},{4,16},{8,28},{12,24},{16,4},{20,0},{24,12},{28,8},{1,21},{... | collective-permute-start | bytes 196616 | tf_op jit(solution)/shard_map/ppermute | solution.py:20
  100.6 10.0 %collective-permute-start.29 = (bf16[64,512]{1,0:T(8,128)(2,1)S(1)}, bf16[64,512]{1,0:T(8,128)(2,1)S(1)}, u32[]{:S(2)}, u32[]{:S(2)}) collective-permute-start(bf16[64,512]{1,0:T(8,128)(2,1)S(1)} %get-tuple-element.46), channel_id=1, source_target_pairs={{0,24},{4,28},{8,16},{12,20},{16,8},{20,12},{24,0},{28,4},{1,25},{... | collective-permute-start | bytes 196616 | tf_op jit(solution)/shard_map/ppermute | solution.py:20
  106.2 5.6 %collective-permute-start.30 = (bf16[64,512]{1,0:T(8,128)(2,1)S(1)}, bf16[64,512]{1,0:T(8,128)(2,1)S(1)}, u32[]{:S(2)}, u32[]{:S(2)}) collective-permute-start(bf16[64,512]{1,0:T(8,128)(2,1)S(1)} %get-tuple-element.45), channel_id=1, source_target_pairs={{0,28},{4,24},{8,20},{12,16},{16,12},{20,8},{24,4},{28,0},{1,29},{... | collective-permute-start | bytes 196616 | tf_op jit(solution)/shard_map/ppermute | solution.py:20
  108.0 3.8 %collective-permute-start.14 = (bf16[64,512]{1,0:T(8,128)(2,1)S(1)}, bf16[64,512]{1,0:T(8,128)(2,1)S(1)}, u32[]{:S(2)}, u32[]{:S(2)}) collective-permute-start(bf16[64,512]{1,0:T(8,128)(2,1)S(1)} %get-tuple-element.51), channel_id=1, source_target_pairs={{0,4},{4,0},{8,12},{12,8},{16,20},{20,16},{24,28},{28,24},{1,5},{5... | collective-permute-start | bytes 196616 | tf_op jit(solution)/shard_map/ppermute | solution.py:20
  108.0 6.5 %copy-start.13 = (bf16[64,512]{1,0:T(8,128)(2,1)}, bf16[64,512]{1,0:T(8,128)(2,1)S(1)}, u32[]{:S(2)}) copy-start(bf16[64,512]{1,0:T(8,128)(2,1)S(1)} %collective-permute-done.27.refs_4_) | copy-start | bytes 196612
  108.0 5.2 %collective-permute-start.15 = (bf16[64,512]{1,0:T(8,128)(2,1)S(1)}, bf16[64,512]{1,0:T(8,128)(2,1)S(1)}, u32[]{:S(2)}, u32[]{:S(2)}) collective-permute-start(bf16[64,512]{1,0:T(8,128)(2,1)S(1)} %get-tuple-element.50), channel_id=1, source_target_pairs={{0,8},{4,12},{8,0},{12,4},{16,24},{20,28},{24,16},{28,20},{1,9},{5... | collective-permute-start | bytes 196616 | tf_op jit(solution)/shard_map/ppermute | solution.py:20
  108.6 5.9 %copy-start.14 = (bf16[64,512]{1,0:T(8,128)(2,1)}, bf16[64,512]{1,0:T(8,128)(2,1)S(1)}, u32[]{:S(2)}) copy-start(bf16[64,512]{1,0:T(8,128)(2,1)S(1)} %collective-permute-done.28.refs_5_) | copy-start | bytes 196612
  108.6 5.8 %collective-permute-start.16 = (bf16[64,512]{1,0:T(8,128)(2,1)S(1)}, bf16[64,512]{1,0:T(8,128)(2,1)S(1)}, u32[]{:S(2)}, u32[]{:S(2)}) collective-permute-start(bf16[64,512]{1,0:T(8,128)(2,1)S(1)} %get-tuple-element.49), channel_id=1, source_target_pairs={{0,12},{4,8},{8,4},{12,0},{16,28},{20,24},{24,20},{28,16},{1,13},{... | collective-permute-start | bytes 196616 | tf_op jit(solution)/shard_map/ppermute | solution.py:20
  110.6 3.9 %copy-start.15 = (bf16[64,512]{1,0:T(8,128)(2,1)}, bf16[64,512]{1,0:T(8,128)(2,1)S(1)}, u32[]{:S(2)}) copy-start(bf16[64,512]{1,0:T(8,128)(2,1)S(1)} %collective-permute-done.29.refs_6_) | copy-start | bytes 196612
  111.8 2.7 %copy-start.16 = (bf16[64,512]{1,0:T(8,128)(2,1)}, bf16[64,512]{1,0:T(8,128)(2,1)S(1)}, u32[]{:S(2)}) copy-start(bf16[64,512]{1,0:T(8,128)(2,1)S(1)} %collective-permute-done.30.refs_7_) | copy-start | bytes 196612
  111.8 2.7 %copy-start.17 = (bf16[64,512]{1,0:T(8,128)(2,1)}, bf16[64,512]{1,0:T(8,128)(2,1)S(1)}, u32[]{:S(2)}) copy-start(bf16[64,512]{1,0:T(8,128)(2,1)S(1)} %collective-permute-done.14.refs_1_) | copy-start | bytes 196612
  113.1 1.3 %copy-start.18 = (bf16[64,512]{1,0:T(8,128)(2,1)}, bf16[64,512]{1,0:T(8,128)(2,1)S(1)}, u32[]{:S(2)}) copy-start(bf16[64,512]{1,0:T(8,128)(2,1)S(1)} %collective-permute-done.15.refs_2_) | copy-start | bytes 196612
  (6 other events, 4.0 us)
